TPU v7x, 32 devices: a whole 2x2x4 slice. The times are simulated.
32 devices in a mesh: sp: 16 (over z, y, x), tp: 2 (over core).
Axes of the slice: x: 2, y: 2, z: 4, core: 2. Of those that a mesh axis runs over, the one named last changes fastest.
Arguments:
- value_in: bfloat16 [4096, 2048], P('sp', 'tp'), may hold values from -25 to 25, as said below
- gate_in: bfloat16 [4096, 2048], P('sp', 'tp'), may hold values from -6 to 6
- taps: float32 [31, 2048], P(None, 'tp'), may hold values from -1 to 1
- gain: float32 [2048], P('tp'), may hold values from 0.1 to 1.9
- shift: float32 [2048], P('tp'), may hold values from -3 to 3
- w_out: bfloat16 [2048, 2048], P('tp'), may hold values from -0.125 to 0.125
- grad_out: bfloat16 [4096, 2048], P('sp'), may hold values from -6 to 6
Outputs:
- d_value: bfloat16 [4096, 2048], P('sp', 'tp')
- d_gate: bfloat16 [4096, 2048], P('sp', 'tp')
- d_taps: float32 [31, 2048], P(None, 'tp')
- d_gain: float32 [2048], P('tp')
- d_shift: float32 [2048], P('tp')
Inputs may be any that keep to these rules, and one draw needn't show every extreme that they name: `value_in`: channel blocks of different magnitude.
All inputs are finite; a program needn't handle non-finite values.
Results may differ from a plain program's by a relative error of at most 0.007.
Values may be sent and summed in bfloat16 or wider, within the bound.
No kernel may reach another device: no remote copies, remote signals or barrier semaphores. Data moves between devices by JAX's collectives and lax.ppermute only.
A program may use at most 64 MiB of HBM per device.

v0:
```python
import math
import jax
import jax.numpy as jnp
from jax import lax
from jax.sharding import PartitionSpec as P

EPS = 1e-05


def with_halo(block, sides, width):
    for axis, dim in sides:
        count = lax.axis_size(axis)
        forward = [(i, i + 1) for i in range(count - 1)]
        backward = [(target, source) for source, target in forward]
        low = lax.ppermute(
            lax.slice_in_dim(block, block.shape[dim] - width, None, axis=dim), axis, forward
        )
        high = lax.ppermute(lax.slice_in_dim(block, 0, width, axis=dim), axis, backward)
        block = jnp.concatenate([low, block, high], axis=dim)
    return block


def gated_rows(value_rows, gate_rows):
    gate_sig = jax.nn.sigmoid(gate_rows.astype(jnp.float32))
    return ((value_rows.astype(jnp.float32) * gate_sig).astype(jnp.bfloat16), gate_sig)


def convolve(window, taps, count):
    wide = window.astype(jnp.float32)
    total = jnp.zeros((count, wide.shape[1]), jnp.float32)
    for offset in range(taps.shape[0]):
        total = total + taps[offset] * wide[offset : offset + count]
    return total


def norm_backward(conv_out, grad_rows, gain, shift, w_out, width):
    sums, squares = lax.psum((jnp.sum(conv_out, 1), jnp.sum(conv_out * conv_out, 1)), "tp")
    mean = sums / width
    var = squares / width - mean * mean
    inv = lax.rsqrt(var + EPS)
    normed = (conv_out - mean[:, None]) * inv[:, None]
    pre = normed * gain + shift
    grad_mix = lax.dot_general(
        grad_rows, w_out, (((1,), (1,)), ((), ())), preferred_element_type=jnp.float32
    )
    sig = jax.nn.sigmoid(pre)
    grad_pre = grad_mix * sig * (1.0 + pre * (1.0 - sig))
    grad_normed = grad_pre * gain
    first, second = lax.psum((jnp.sum(grad_normed, 1), jnp.sum(grad_normed * normed, 1)), "tp")
    grad_conv = inv[:, None] * (
        grad_normed - first[:, None] / width - normed * second[:, None] / width
    )
    return (grad_conv, grad_pre, normed)


def shards(value_in, gate_in, taps, gain, shift, w_out, grad_out):
    half = taps.shape[0] // 2
    kernel = taps.shape[0]
    rows = value_in.shape[0]
    width = value_in.shape[1] * lax.axis_size("tp")
    total = rows * lax.axis_size("sp")
    gated, gate_sig = gated_rows(value_in, gate_in)
    gated_wide = with_halo(gated, (("sp", 0),), half)
    conv_out = convolve(gated_wide, taps, rows)
    grad_conv, grad_pre, normed = norm_backward(conv_out, grad_out, gain, shift, w_out, width)
    grad_wide = with_halo(grad_conv, (("sp", 0),), half)
    own_grad = grad_wide[half : half + rows]
    gated_float = gated_wide.astype(jnp.float32)
    grad_gated = jnp.zeros((rows, own_grad.shape[1]), jnp.float32)
    for offset in range(kernel):
        grad_gated = (
            grad_gated + taps[offset] * grad_wide[2 * half - offset : 2 * half - offset + rows]
        )
    tap_terms = jnp.stack(
        [jnp.sum(own_grad * gated_float[offset : offset + rows], 0) for offset in range(kernel)]
    )
    scale = 1.0 / math.sqrt(total)
    stacked = (
        jnp.concatenate(
            [tap_terms, jnp.sum(grad_pre * normed, 0)[None], jnp.sum(grad_pre, 0)[None]], 0
        )
        * scale
    )
    summed = lax.psum(stacked, "sp")
    d_taps = summed[:kernel]
    d_gain = summed[kernel]
    d_shift = summed[kernel + 1]
    d_value = (grad_gated * gate_sig).astype(jnp.bfloat16)
    d_gate = (grad_gated * value_in.astype(jnp.float32) * gate_sig * (1.0 - gate_sig)).astype(
        jnp.bfloat16
    )
    return (d_value, d_gate, d_taps, d_gain, d_shift)


def solution(mesh):
    return jax.shard_map(
        shards,
        mesh=mesh,
        in_specs=(
            P("sp", "tp"),
            P("sp", "tp"),
            P(None, "tp"),
            P("tp"),
            P("tp"),
            P("tp", None),
            P("sp", None),
        ),
        out_specs=(P("sp", "tp"), P("sp", "tp"), P(None, "tp"), P("tp"), P("tp")),
        check_vma=False,
    )
```

profile of v0, /device:TPU:0, one launch (start us, length us, event | category | flops | bytes accessed | tf_op | source)
XLA Modules:
  0.0 175.2 jit_solution(298959568165321427)
XLA Ops:
  7.2 0.0 copy-start
  7.2 0.0 copy-start.4
  7.2 0.0 all-reduce.4.cloned.1.call-start
  7.2 1.6 fusion.1
  8.9 4.9 %collective-permute-start = (bf16[15,1024]{1,0:T(8,128)(2,1)S(1)}, bf16[15,1024]{1,0:T(8,128)(2,1)S(1)}, u32[]{:S(2)}, u32[]{:S(2)}) collective-permute-start(bf16[15,1024]{1,0:T(8,128)(2,1)S(1)} %get-tuple-element.52), channel_id=1, source_target_pairs={{0,2},{2,4},{4,6},{6,8},{8,10},{10,12},{12,14},{14,16},{16,18},{18... | collective-permute-start | bytes 92168 | tf_op jit(solution)/shard_map/ppermute | solution.py:15
  13.7 1.3 collective-permute-start.1
  15.0 0.0 copy-done.4
  15.0 0.1 fusion.97
  15.1 0.0 copy-start.5
  15.1 0.0 copy-start.6
  15.1 0.0 copy-start.7
  15.1 0.0 copy-start.8
  15.1 0.0 copy-start.9
  15.2 0.0 copy-start.10
  15.2 0.0 copy-start.11
  15.2 0.0 copy-start.12
  15.2 0.0 copy-start.13
  15.2 0.0 copy-start.14
  15.3 0.0 copy-start.15
  15.3 0.0 copy-start.16
  15.3 0.0 copy-start.17
  15.3 0.0 copy-start.18
  15.3 0.0 copy-start.19
  15.3 0.0 collective-permute-done
  15.4 4.2 %collective-permute-done.1 = bf16[15,1024]{1,0:T(8,128)(2,1)S(1)} collective-permute-done((bf16[15,1024]{1,0:T(8,128)(2,1)S(1)}, bf16[15,1024]{1,0:T(8,128)(2,1)S(1)}, u32[]{:S(2)}, u32[]{:S(2)}) %collective-permute-start.1) | collective-permute-done | bytes 30752 | tf_op jit(solution)/shard_map/ppermute | solution.py:18
  19.5 0.2 maximum_convert_fusion
  19.7 0.0 copy-start.24
  19.7 0.0 copy-start.25
  19.7 5.7 %multiply_reduce_fusion.33 = (f32[256]{0:T(256)S(1)}, f32[256]{0:T(256)S(1)}, f32[256,1024]{1,0:T(8,128)S(1)}) fusion(f32[286,1024]{1,0:T(8,128)S(1)} %maximum_convert_fusion, f32[1024]{0:T(1024)S(1)} %bitcast.126, f32[1024]{0:T(1024)S(1)} %bitcast.128, f32[1024]{0:T(1024)S(1)} %bitcast.70, f32[1024]{0:T(1024)S(1)} %bitcast.72, f32[1024]{0:T(1024)S(1)} %bitcast.74, ...), kind=kLoop, calls=%fused_computation.186 | loop fusion | flops 16776704 | bytes 33683456 | tf_op jit(solution)/shard_map/reduce_sum | solution.py:37
  25.6 2.5 %all-reduce.1 = (f32[256]{0:T(256)S(1)}, f32[256]{0:T(256)S(1)}) all-reduce(f32[256]{0:T(256)S(1)} %get-tuple-element.41, f32[256]{0:T(256)S(1)} %get-tuple-element.40), channel_id=1, replica_groups=mesh['sp'=16,'tp'=2] {'tp'}, use_global_device_ids=true, to_apply=%region_3.0 | all-reduce | flops 512 | bytes 4096 | tf_op jit(solution)/shard_map/psum | solution.py:37
  28.1 0.0 copy-done
  28.1 5.5 %multiply_reduce_fusion = (f32[1024]{0:T(1024)}, f32[256]{0:T(256)S(1)}, f32[256]{0:T(256)S(1)}, f32[1024]{0:T(1024)}, f32[256,1024]{1,0:T(8,128)}) fusion(f32[256,1024]{1,0:T(8,128)S(1)} %get-tuple-element.49, f32[256]{0:T(256)S(1)} %get-tuple-element.88, f32[256]{0:T(256)S(1)} %get-tuple-element.87, f32[1024]{0:T(1024)S(1)} %copy-done.24, ...), kind=kOutput, calls=%fused_computation.150 | convolution fusion | flops 1078720000 | bytes 7360512 | tf_op jit(solution)/shard_map/dot_general | solution.py:43
  33.7 2.4 %all-reduce = (f32[256]{0:T(256)S(1)}, f32[256]{0:T(256)S(1)}) all-reduce(f32[256]{0:T(256)S(1)} %get-tuple-element.37, f32[256]{0:T(256)S(1)} %get-tuple-element.38), channel_id=1, replica_groups=mesh['sp'=16,'tp'=2] {'tp'}, use_global_device_ids=true, to_apply=%region_7.0 | all-reduce | flops 512 | bytes 4096 | tf_op jit(solution)/shard_map/psum | solution.py:49
  36.1 4.8 %multiply_reduce_fusion.1 = (f32[1024]{0:T(1024)}, f32[1024]{0:T(1024)}, f32[1024]{0:T(1024)}, f32[1024]{0:T(1024)}, f32[1024]{0:T(1024)}, /*index=5*/f32[1024]{...) fusion(f32[286,1024]{1,0:T(8,128)S(1)} %maximum_convert_fusion,, ...), kind=kLoop, calls=%fused_computation.151 | loop fusion | flops 11515904 | bytes 22102016 | tf_op jit(solution)/shard_map/reduce_sum | solution.py:75
  41.0 2.4 %multiply_reduce_fusion.2 = (f32[1024]{0:T(1024)}, f32[1024]{0:T(1024)}, f32[1024]{0:T(1024)}, f32[1024]{0:T(1024)}, f32[1024]{0:T(1024)}, /*index=5*/f32[1024]{...) fusion(f32[256,1024]{1,0:T(8,128)S(1)} %get-tuple-element.46, ...), kind=kLoop, calls=%fused_computation.152 | loop fusion | flops 6802432 | bytes 14733312 | tf_op jit(solution)/shard_map/reduce_sum | solution.py:75
  43.3 0.6 fusion.94
  44.0 1.3 collective-permute-start.2
  45.3 4.9 %collective-permute-start.3 = (f32[15,1024]{1,0:T(8,128)S(1)}, f32[15,1024]{1,0:T(8,128)S(1)}, u32[]{:S(2)}, u32[]{:S(2)}) collective-permute-start(f32[15,1024]{1,0:T(8,128)S(1)} %get-tuple-element.51), channel_id=1, source_target_pairs={{0,2},{2,4},{4,6},{6,8},{8,10},{10,12},{12,14},{14,16},{16,18},{18... | collective-permute-start | bytes 184328 | tf_op jit(solution)/shard_map/ppermute | solution.py:15
  50.2 3.8 %concatenate.44 = f32[33,1024]{1,0:T(8,128)S(1)} concatenate(f32[1,1024]{1,0:T(1,128)} %bitcast.160, f32[1,1024]{1,0:T(1,128)} %bitcast.159, f32[1,1024]{1,0:T(1,128)} %bitcast.158, f32[1,1024]{1,0:T(1,128)} %bitcast.157, f32[1,1024]{1,0:T(1,128)} %bitcast.156, f32[1,1024]{1,0:T(1,128)} %bitcast.155, f32[1,1024]{1,0:T(1,128)} %bitcast.154, f32[1,1024]{1,0:T(1,128)} %bitcast.153, ...), dimensions={0} | concatenate | bytes 270336 | tf_op jit(solution)/shard_map/concatenate | solution.py:79
  54.0 0.7 broadcast_multiply_fusion
  54.7 0.0 all-reduce.4.cloned.1.call-update
  54.7 0.0 collective-permute-done.2
  54.7 0.0 collective-permute-done.3
  54.8 6.9 %fusion.4 = (bf16[256,1024]{1,0:T(8,128)(2,1)}, f32[256,1024]{1,0:T(8,128)}) fusion(bf16[256,1024]{1,0:T(8,128)(2,1)S(1)} %copy-done.3, bf16[256,1024]{1,0:T(8,128)(2,1)S(1)} %copy-done.1, f32[256,1024]{1,0:T(8,128)S(1)} %get-tuple-element.46, f32[15,1024]{1,0:T(8,128)S(1)} %collective-permute-done.3, f32[1024]{0:T(1024)} %bitcast.127, f32[1024]{0:T(1024)} %bitcast.129, ...), kind=kLoop, calls=%fused_computation.35 | loop fusion | flops 26476544 | bytes 3919872 | tf_op jit(solution)/shard_map/convert_element_type | solution.py:89
  61.7 2.3 %multiply_convert_fusion = bf16[256,1024]{1,0:T(8,128)(2,1)} fusion(f32[256,1024]{1,0:T(8,128)} %get-tuple-element.48, bf16[256,1024]{1,0:T(8,128)(2,1)S(1)} %copy-done.1), kind=kLoop, calls=%fused_computation.182 | loop fusion | flops 1572864 | bytes 2097152 | tf_op jit(solution)/shard_map/convert_element_type | solution.py:88
  64.0 101.4 %all-reduce.4.cloned.1.call-done = f32[33,1024]{1,0:T(8,128)} async-done(((f32[33,1024]{1,0:T(8,128)}), f32[33,1024]{1,0:T(8,128)}) %all-reduce.4.cloned.1.call-update) | async-done | bytes 135184 | tf_op jit(solution)/shard_map/psum | solution.py:84
  165.4 1.4 fusion.96
  166.8 1.6 slice.579
  (35 shorter events, 0.1 us)
Async XLA Ops:
  7.2 20.9 %copy-start = (bf16[256,2048]{1,0:T(8,128)(2,1)S(1)}, bf16[256,2048]{1,0:T(8,128)(2,1)}, u32[]{:S(2)}) copy-start(bf16[256,2048]{1,0:T(8,128)(2,1)} %param.13) | copy-start | bytes 3145732
  7.2 7.9 %copy-start.4 = (f32[31,1024]{1,0:T(8,128)S(1)}, f32[31,1024]{1,0:T(8,128)}, u32[]{:S(2)}) copy-start(f32[31,1024]{1,0:T(8,128)} %param.9) | copy-start | bytes 380932
  7.2 158.2 %all-reduce.4.cloned.1.call-start = ((), (), s32[]{:S(2)}) async-start(), calls=%async_computation | async-start | bytes 327680 | tf_op jit(solution)/shard_map/psum | solution.py:84
  8.9 6.5 %collective-permute-start = (bf16[15,1024]{1,0:T(8,128)(2,1)S(1)}, bf16[15,1024]{1,0:T(8,128)(2,1)S(1)}, u32[]{:S(2)}, u32[]{:S(2)}) collective-permute-start(bf16[15,1024]{1,0:T(8,128)(2,1)S(1)} %get-tuple-element.52), channel_id=1, source_target_pairs={{0,2},{2,4},{4,6},{6,8},{8,10},{10,12},{12,14},{14,16},{16,18},{18... | collective-permute-start | bytes 92168 | tf_op jit(solution)/shard_map/ppermute | solution.py:15
  13.7 5.8 %collective-permute-start.1 = (bf16[15,1024]{1,0:T(8,128)(2,1)S(1)}, bf16[15,1024]{1,0:T(8,128)(2,1)S(1)}, u32[]{:S(2)}, u32[]{:S(2)}) collective-permute-start(bf16[15,1024]{1,0:T(8,128)(2,1)S(1)} %get-tuple-element.53), channel_id=1, source_target_pairs={{2,0},{4,2},{6,4},{8,6},{10,8},{12,10},{14,12},{16,14},{18,16},{20... | collective-permute-start | bytes 92168 | tf_op jit(solution)/shard_map/ppermute | solution.py:18
  15.1 10.3 %copy-start.5 = (f32[1,1024]{1,0:T(1,128)}, f32[1,1024]{1,0:T(1,128)S(1)}, u32[]{:S(2)}) copy-start(f32[1,1024]{1,0:T(1,128)S(1)} %get-tuple-element.68) | copy-start | bytes 12292
  15.1 10.3 %copy-start.6 = (f32[1,1024]{1,0:T(1,128)}, f32[1,1024]{1,0:T(1,128)S(1)}, u32[]{:S(2)}) copy-start(f32[1,1024]{1,0:T(1,128)S(1)} %get-tuple-element.69) | copy-start | bytes 12292
  15.1 10.3 %copy-start.7 = (f32[1,1024]{1,0:T(1,128)}, f32[1,1024]{1,0:T(1,128)S(1)}, u32[]{:S(2)}) copy-start(f32[1,1024]{1,0:T(1,128)S(1)} %get-tuple-element.70) | copy-start | bytes 12292
  15.1 10.3 %copy-start.8 = (f32[1,1024]{1,0:T(1,128)}, f32[1,1024]{1,0:T(1,128)S(1)}, u32[]{:S(2)}) copy-start(f32[1,1024]{1,0:T(1,128)S(1)} %get-tuple-element.71) | copy-start | bytes 12292
  15.1 10.3 %copy-start.9 = (f32[1,1024]{1,0:T(1,128)}, f32[1,1024]{1,0:T(1,128)S(1)}, u32[]{:S(2)}) copy-start(f32[1,1024]{1,0:T(1,128)S(1)} %get-tuple-element.72) | copy-start | bytes 12292
  15.2 10.3 %copy-start.10 = (f32[1,1024]{1,0:T(1,128)}, f32[1,1024]{1,0:T(1,128)S(1)}, u32[]{:S(2)}) copy-start(f32[1,1024]{1,0:T(1,128)S(1)} %get-tuple-element.73) | copy-start | bytes 12292
  15.2 10.3 %copy-start.11 = (f32[1,1024]{1,0:T(1,128)}, f32[1,1024]{1,0:T(1,128)S(1)}, u32[]{:S(2)}) copy-start(f32[1,1024]{1,0:T(1,128)S(1)} %get-tuple-element.74) | copy-start | bytes 12292
  15.2 10.3 %copy-start.12 = (f32[1,1024]{1,0:T(1,128)}, f32[1,1024]{1,0:T(1,128)S(1)}, u32[]{:S(2)}) copy-start(f32[1,1024]{1,0:T(1,128)S(1)} %get-tuple-element.75) | copy-start | bytes 12292
  15.2 10.3 %copy-start.13 = (f32[1,1024]{1,0:T(1,128)}, f32[1,1024]{1,0:T(1,128)S(1)}, u32[]{:S(2)}) copy-start(f32[1,1024]{1,0:T(1,128)S(1)} %get-tuple-element.76) | copy-start | bytes 12292
  15.2 10.3 %copy-start.14 = (f32[1,1024]{1,0:T(1,128)}, f32[1,1024]{1,0:T(1,128)S(1)}, u32[]{:S(2)}) copy-start(f32[1,1024]{1,0:T(1,128)S(1)} %get-tuple-element.77) | copy-start | bytes 12292
  15.3 10.3 %copy-start.15 = (f32[1,1024]{1,0:T(1,128)}, f32[1,1024]{1,0:T(1,128)S(1)}, u32[]{:S(2)}) copy-start(f32[1,1024]{1,0:T(1,128)S(1)} %get-tuple-element.78) | copy-start | bytes 12292
  15.3 10.3 %copy-start.16 = (f32[1,1024]{1,0:T(1,128)}, f32[1,1024]{1,0:T(1,128)S(1)}, u32[]{:S(2)}) copy-start(f32[1,1024]{1,0:T(1,128)S(1)} %get-tuple-element.79) | copy-start | bytes 12292
  15.3 10.3 %copy-start.17 = (f32[1,1024]{1,0:T(1,128)}, f32[1,1024]{1,0:T(1,128)S(1)}, u32[]{:S(2)}) copy-start(f32[1,1024]{1,0:T(1,128)S(1)} %get-tuple-element.80) | copy-start | bytes 12292
  15.3 10.3 %copy-start.18 = (f32[1,1024]{1,0:T(1,128)}, f32[1,1024]{1,0:T(1,128)S(1)}, u32[]{:S(2)}) copy-start(f32[1,1024]{1,0:T(1,128)S(1)} %get-tuple-element.81) | copy-start | bytes 12292
  15.3 10.3 %copy-start.19 = (f32[1,1024]{1,0:T(1,128)}, f32[1,1024]{1,0:T(1,128)S(1)}, u32[]{:S(2)}) copy-start(f32[1,1024]{1,0:T(1,128)S(1)} %get-tuple-element.82) | copy-start | bytes 12292
  15.3 10.3 %copy-start.20 = (f32[1,1024]{1,0:T(1,128)}, f32[1,1024]{1,0:T(1,128)S(1)}, u32[]{:S(2)}) copy-start(f32[1,1024]{1,0:T(1,128)S(1)} %get-tuple-element.83) | copy-start | bytes 12292
  15.3 10.3 %copy-start.21 = (f32[1,1024]{1,0:T(1,128)}, f32[1,1024]{1,0:T(1,128)S(1)}, u32[]{:S(2)}) copy-start(f32[1,1024]{1,0:T(1,128)S(1)} %get-tuple-element.84) | copy-start | bytes 12292
  15.3 10.3 %copy-start.22 = (f32[1,1024]{1,0:T(1,128)}, f32[1,1024]{1,0:T(1,128)S(1)}, u32[]{:S(2)}) copy-start(f32[1,1024]{1,0:T(1,128)S(1)} %get-tuple-element.85) | copy-start | bytes 12292
  15.3 10.3 %copy-start.23 = (f32[1,1024]{1,0:T(1,128)}, f32[1,1024]{1,0:T(1,128)S(1)}, u32[]{:S(2)}) copy-start(f32[1,1024]{1,0:T(1,128)S(1)} %get-tuple-element.86) | copy-start | bytes 12292
  19.7 8.4 %copy-start.24 = (f32[1024]{0:T(1024)S(1)}, f32[1024]{0:T(1024)}, u32[]{:S(2)}) copy-start(f32[1024]{0:T(1024)} %param.10) | copy-start | bytes 12292
  19.7 8.4 %copy-start.25 = (f32[1024]{0:T(1024)S(1)}, f32[1024]{0:T(1024)}, u32[]{:S(2)}) copy-start(f32[1024]{0:T(1024)} %param.11) | copy-start | bytes 12292
  25.6 8.0 %copy-start.2 = (f32[256,1024]{1,0:T(8,128)}, f32[256,1024]{1,0:T(8,128)S(1)}, u32[]{:S(2)}) copy-start(f32[256,1024]{1,0:T(8,128)S(1)} %get-tuple-element.49) | copy-start | bytes 3145732
  43.3 11.4 %copy-start.1 = (bf16[256,1024]{1,0:T(8,128)(2,1)S(1)}, bf16[256,1024]{1,0:T(8,128)(2,1)}, u32[]{:S(2)}) copy-start(bf16[256,1024]{1,0:T(8,128)(2,1)} %param.8) | copy-start | bytes 1572868
  43.3 11.4 %copy-start.3 = (bf16[256,1024]{1,0:T(8,128)(2,1)S(1)}, bf16[256,1024]{1,0:T(8,128)(2,1)}, u32[]{:S(2)}) copy-start(bf16[256,1024]{1,0:T(8,128)(2,1)} %param.7) | copy-start | bytes 1572868
  44.0 10.7 %collective-permute-start.2 = (f32[15,1024]{1,0:T(8,128)}, f32[15,1024]{1,0:T(8,128)S(1)}, u32[]{:S(2)}, u32[]{:S(2)}) collective-permute-start(f32[15,1024]{1,0:T(8,128)} %get-tuple-element.50), channel_id=1, source_target_pairs={{2,0},{4,2},{6,4},{8,6},{10,8},{12,10},{14,12},{16,14},{18,16},{20... | collective-permute-start | bytes 184328 | tf_op jit(solution)/shard_map/ppermute | solution.py:18
  45.3 9.5 %collective-permute-start.3 = (f32[15,1024]{1,0:T(8,128)S(1)}, f32[15,1024]{1,0:T(8,128)S(1)}, u32[]{:S(2)}, u32[]{:S(2)}) collective-permute-start(f32[15,1024]{1,0:T(8,128)S(1)} %get-tuple-element.51), channel_id=1, source_target_pairs={{0,2},{2,4},{4,6},{6,8},{8,10},{10,12},{12,14},{14,16},{16,18},{18... | collective-permute-start | bytes 184328 | tf_op jit(solution)/shard_map/ppermute | solution.py:15
Sparse Core Ops, SparseCore 0:
  54.8 110.4 all-reduce.3
where the time goes:
time: 176 us; the launch traced here: 175 us
  waiting for transfers between devices  106 us (60%)
  other arithmetic  24.5 us (14%)
  between operations  14.5 us (8%)
  starting transfers between devices  12.4 us (7%)
  local copies, waits for them, and re-layouts  7.63 us (4%)
  matrix products  5.53 us (3%)
  blocking collectives  4.91 us (3%)
    psum x1, waiting for transfers between devices, shards(): summed = lax.psum(stacked, 'sp')  101 us
    ppermute x2, starting transfers between devices, with_halo(): lax.ppermute(lax.slice_in_dim(block, block.shape[dim] - width, None, axis...  9.8 us
    reduce_sum x2, other arithmetic, shards(): jnp.sum(own_grad * gated_float[offset:offset + rows], 0)  7.23 us
    convert_element_type x1, other arithmetic, shards(): (grad_gated * value_in.astype(jnp.float32) * gate_sig * (1.0 - gate_sig))...  6.89 us
    reduce_sum x1, other arithmetic, norm_backward(): jnp.sum(conv_out * conv_out, 1)  5.69 us
    dot_general x1, matrix products, norm_backward(): lax.dot_general(grad_rows, w_out, (((1,), (1,)), ((), ())), preferred_ele...  5.53 us
    ppermute x2, waiting for transfers between devices, with_halo(): lax.ppermute(lax.slice_in_dim(block, 0, width, axis=dim), axis, backward)  4.19 us
    concatenate x1, local copies, waits for them, and re-layouts, shards(): jnp.concatenate([tap_terms, jnp.sum(grad_pre * normed, 0)[None], jnp.sum(...  3.82 us
  transfers between devices with their start and end apart: 5, of which 2 were waited for; matrix products, arithmetic and copies ran while one was open for 8% of the time, Pallas kernels for 0%

commit v1 on v0

--- a/solution.py
+++ b/solution.py
@@ -5,6 +5,14 @@
 from jax.sharding import PartitionSpec as P
 
 EPS = 1e-05
+
+
+def doubling_sum(x, name):
+    size, total = (lax.axis_size(name), x)
+    for far in [1 << k for k in range(size.bit_length() - 1)]:
+        swap = [(i, i ^ far) for i in range(size)]
+        total = total + lax.ppermute(total, name, swap)
+    return total
 
 
 def with_halo(block, sides, width):
@@ -81,7 +89,7 @@
         )
         * scale
     )
-    summed = lax.psum(stacked, "sp")
+    summed = doubling_sum(stacked, "sp")
     d_taps = summed[:kernel]
     d_gain = summed[kernel]
     d_shift = summed[kernel + 1]

time: 176 us -> 78.8 us (0.45)
  waiting for transfers between devices: 106 us -> 12.6 us
  between operations: 14.5 us -> 0.86 us
  starting transfers between devices: 12.4 us -> 24.5 us
  local copies, waits for them, and re-layouts: 7.63 us -> 5.38 us
    psum x1 -> x0, waiting for transfers between devices: 101 us -> none  [shards(): summed = lax.psum(stacked, 'sp')]
    ppermute x0 -> x4, starting transfers between devices: none -> 12.5 us  [doubling_sum(): total = total + lax.ppermute(total, name, swap)]
    ppermute x0 -> x4, waiting for transfers between devices: none -> 7.99 us  [doubling_sum(): total = total + lax.ppermute(total, name, swap)]
  transfers between devices with their start and end apart: 5 -> 8, of which waited for: 2 -> 5; matrix products, arithmetic and copies ran while one was open for 8% -> 11% of each run, Pallas kernels for 0% -> 0%
where the time goes in v1:
time: 78.8 us; the launch traced here: 78.3 us
  other arithmetic  24.6 us (31%)
  starting transfers between devices  24.5 us (31%)
  waiting for transfers between devices  12.6 us (16%)
  matrix products  5.53 us (7%)
  local copies, waits for them, and re-layouts  5.38 us (7%)
  blocking collectives  4.91 us (6%)
  between operations  0.86 us (1%)
    ppermute x4, starting transfers between devices, doubling_sum(): total = total + lax.ppermute(total, name, swap)  12.5 us
    ppermute x2, starting transfers between devices, with_halo(): lax.ppermute(lax.slice_in_dim(block, block.shape[dim] - width, None, axis...  9.42 us
    ppermute x4, waiting for transfers between devices, doubling_sum(): total = total + lax.ppermute(total, name, swap)  7.99 us
    reduce_sum x2, other arithmetic, shards(): jnp.sum(own_grad * gated_float[offset:offset + rows], 0)  7.23 us
    convert_element_type x1, other arithmetic, shards(): (grad_gated * value_in.astype(jnp.float32) * gate_sig * (1.0 - gate_sig))...  6.57 us
    reduce_sum x1, other arithmetic, norm_backward(): jnp.sum(conv_out * conv_out, 1)  5.69 us
    dot_general x1, matrix products, norm_backward(): lax.dot_general(grad_rows, w_out, (((1,), (1,)), ((), ())), preferred_ele...  5.53 us
    ppermute x2, waiting for transfers between devices, with_halo(): lax.ppermute(lax.slice_in_dim(block, 0, width, axis=dim), axis, backward)  4.23 us
  transfers between devices with their start and end apart: 8, of which 5 were waited for; matrix products, arithmetic and copies ran while one was open for 11% of the time, Pallas kernels for 0%

profile of v1, /device:TPU:0, one launch (start us, length us, event | category | flops | bytes accessed | tf_op | source)
XLA Modules:
  0.0 78.3 jit_solution(14285861433512021233)
XLA Ops:
  0.6 0.0 copy-start
  0.6 0.0 copy-start.4
  0.7 1.6 %fusion.1 = bf16[256,1024]{1,0:T(8,128)(2,1)S(1)} fusion(bf16[256,1024]{1,0:T(8,128)(2,1)} %param.7, bf16[256,1024]{1,0:T(8,128)(2,1)} %param.8), kind=kLoop, calls=%fused_computation.32 | loop fusion | flops 1835008 | bytes 1572864 | tf_op jit(solution)/shard_map/convert_element_type | solution.py:33
  2.3 4.9 %collective-permute-start = (bf16[15,1024]{1,0:T(8,128)(2,1)S(1)}, bf16[15,1024]{1,0:T(8,128)(2,1)S(1)}, u32[]{:S(2)}, u32[]{:S(2)}) collective-permute-start(bf16[15,1024]{1,0:T(8,128)(2,1)S(1)} %get-tuple-element.52), channel_id=1, source_target_pairs={{0,2},{2,4},{4,6},{6,8},{8,10},{10,12},{12,14},{14,16},{16,18},{18... | collective-permute-start | bytes 92168 | tf_op jit(solution)/shard_map/ppermute | solution.py:23
  7.2 1.3 %collective-permute-start.1 = (bf16[15,1024]{1,0:T(8,128)(2,1)S(1)}, bf16[15,1024]{1,0:T(8,128)(2,1)S(1)}, u32[]{:S(2)}, u32[]{:S(2)}) collective-permute-start(bf16[15,1024]{1,0:T(8,128)(2,1)S(1)} %get-tuple-element.53), channel_id=1, source_target_pairs={{2,0},{4,2},{6,4},{8,6},{10,8},{12,10},{14,12},{16,14},{18,16},{20... | collective-permute-start | bytes 92168 | tf_op jit(solution)/shard_map/ppermute | solution.py:26
  8.5 0.0 copy-done.4
  8.5 0.1 fusion.98
  8.6 0.0 copy-start.5
  8.6 0.0 copy-start.6
  8.6 0.0 copy-start.7
  8.6 0.1 collective-permute-done
  8.8 4.2 %collective-permute-done.1 = bf16[15,1024]{1,0:T(8,128)(2,1)S(1)} collective-permute-done((bf16[15,1024]{1,0:T(8,128)(2,1)S(1)}, bf16[15,1024]{1,0:T(8,128)(2,1)S(1)}, u32[]{:S(2)}, u32[]{:S(2)}) %collective-permute-start.1) | collective-permute-done | bytes 30752 | tf_op jit(solution)/shard_map/ppermute | solution.py:26
  13.0 0.2 maximum_convert_fusion
  13.1 0.0 copy-start.8
  13.2 0.0 copy-start.9
  13.2 5.7 %multiply_reduce_fusion.33 = (f32[256]{0:T(256)S(1)}, f32[256]{0:T(256)S(1)}, f32[256,1024]{1,0:T(8,128)S(1)}) fusion(f32[286,1024]{1,0:T(8,128)S(1)} %maximum_convert_fusion, f32[1024]{0:T(1024)S(1)} %bitcast.126, f32[1024]{0:T(1024)S(1)} %bitcast.128, f32[1024]{0:T(1024)S(1)} %bitcast.70, f32[1024]{0:T(1024)S(1)} %bitcast.72, f32[1024]{0:T(1024)S(1)} %bitcast.74, ...), kind=kLoop, calls=%fused_computation.186 | loop fusion | flops 16776704 | bytes 33683456 | tf_op jit(solution)/shard_map/reduce_sum | solution.py:45
  18.9 0.0 copy-done.5
  18.9 0.0 copy-done.6
  18.9 0.0 copy-done.7
  18.9 0.0 copy-start.2
  18.9 2.5 %all-reduce.1 = (f32[256]{0:T(256)S(1)}, f32[256]{0:T(256)S(1)}) all-reduce(f32[256]{0:T(256)S(1)} %get-tuple-element.41, f32[256]{0:T(256)S(1)} %get-tuple-element.40), channel_id=1, replica_groups=mesh['sp'=16,'tp'=2] {'tp'}, use_global_device_ids=true, to_apply=%region_3.0 | all-reduce | flops 512 | bytes 4096 | tf_op jit(solution)/shard_map/psum | solution.py:45
  21.4 0.0 copy-done
  21.4 0.0 copy-done.8
  21.4 0.0 copy-done.9
  21.4 5.5 %multiply_reduce_fusion = (f32[1024]{0:T(1024)}, f32[256]{0:T(256)S(1)}, f32[256]{0:T(256)S(1)}, f32[1024]{0:T(1024)}, f32[256,1024]{1,0:T(8,128)}) fusion(f32[256,1024]{1,0:T(8,128)S(1)} %get-tuple-element.49, f32[256]{0:T(256)S(1)} %get-tuple-element.88, f32[256]{0:T(256)S(1)} %get-tuple-element.87, f32[1024]{0:T(1024)S(1)} %copy-done.8, ...), kind=kOutput, calls=%fused_computation.150 | convolution fusion | flops 1078720000 | bytes 7360512 | tf_op jit(solution)/shard_map/dot_general | solution.py:51
  26.9 0.0 copy-done.2
  26.9 2.4 %all-reduce = (f32[256]{0:T(256)S(1)}, f32[256]{0:T(256)S(1)}) all-reduce(f32[256]{0:T(256)S(1)} %get-tuple-element.37, f32[256]{0:T(256)S(1)} %get-tuple-element.38), channel_id=1, replica_groups=mesh['sp'=16,'tp'=2] {'tp'}, use_global_device_ids=true, to_apply=%region_7.0 | all-reduce | flops 512 | bytes 4096 | tf_op jit(solution)/shard_map/psum | solution.py:57
  29.4 4.8 %multiply_reduce_fusion.1 = (f32[1024]{0:T(1024)}, f32[1024]{0:T(1024)}, f32[1024]{0:T(1024)}, f32[1024]{0:T(1024)}, f32[1024]{0:T(1024)}, /*index=5*/f32[1024]{...) fusion(f32[286,1024]{1,0:T(8,128)S(1)} %maximum_convert_fusion,, ...), kind=kLoop, calls=%fused_computation.151 | loop fusion | flops 11515904 | bytes 22102016 | tf_op jit(solution)/shard_map/reduce_sum | solution.py:83
  34.2 2.4 %multiply_reduce_fusion.2 = (f32[1024]{0:T(1024)}, f32[1024]{0:T(1024)}, f32[1024]{0:T(1024)}, f32[1024]{0:T(1024)}, f32[1024]{0:T(1024)}, /*index=5*/f32[1024]{...) fusion(f32[256,1024]{1,0:T(8,128)S(1)} %get-tuple-element.46, ...), kind=kLoop, calls=%fused_computation.152 | loop fusion | flops 6802432 | bytes 14733312 | tf_op jit(solution)/shard_map/reduce_sum | solution.py:83
  36.6 3.9 %concatenate.44 = f32[33,1024]{1,0:T(8,128)S(1)} concatenate(f32[1,1024]{1,0:T(1,128)} %bitcast.160, f32[1,1024]{1,0:T(1,128)} %bitcast.159, f32[1,1024]{1,0:T(1,128)} %bitcast.158, f32[1,1024]{1,0:T(1,128)} %bitcast.157, f32[1,1024]{1,0:T(1,128)} %bitcast.156, f32[1,1024]{1,0:T(1,128)} %bitcast.155, f32[1,1024]{1,0:T(1,128)} %bitcast.154, f32[1,1024]{1,0:T(1,128)} %bitcast.153, ...), dimensions={0} | concatenate | bytes 270336 | tf_op jit(solution)/shard_map/concatenate | solution.py:87
  40.6 2.5 %collective-permute-start.4 = (f32[33,1024]{1,0:T(8,128)S(1)}, f32[33,1024]{1,0:T(8,128)S(1)}, u32[]{:S(2)}, u32[]{:S(2)}) collective-permute-start(f32[33,1024]{1,0:T(8,128)S(1)} %broadcast_multiply_fusion), channel_id=1, source_target_pairs={{0,2},{2,0},{4,6},{6,4},{8,10},{10,8},{12,14},{14,12},{16,18},{18,... | collective-permute-start | bytes 405512 | tf_op jit(solution)/shard_map/ppermute | solution.py:14
  43.0 4.5 %collective-permute-done.4 = f32[33,1024]{1,0:T(8,128)S(1)} collective-permute-done((f32[33,1024]{1,0:T(8,128)S(1)}, f32[33,1024]{1,0:T(8,128)S(1)}, u32[]{:S(2)}, u32[]{:S(2)}) %collective-permute-start.4) | collective-permute-done | bytes 135200 | tf_op jit(solution)/shard_map/ppermute | solution.py:14
  47.6 2.5 %collective-permute-start.5 = (f32[33,1024]{1,0:T(8,128)S(1)}, f32[33,1024]{1,0:T(8,128)S(1)}, u32[]{:S(2)}, u32[]{:S(2)}) collective-permute-start(f32[33,1024]{1,0:T(8,128)S(1)} %fusion.93), channel_id=1, source_target_pairs={{0,4},{2,6},{4,0},{6,2},{8,12},{10,14},{12,8},{14,10},{16,20},{18,... | collective-permute-start | bytes 405512 | tf_op jit(solution)/shard_map/ppermute | solution.py:14
  50.1 1.3 %collective-permute-start.2 = (f32[15,1024]{1,0:T(8,128)S(1)}, f32[15,1024]{1,0:T(8,128)S(1)}, u32[]{:S(2)}, u32[]{:S(2)}) collective-permute-start(f32[15,1024]{1,0:T(8,128)S(1)} %get-tuple-element.50), channel_id=1, source_target_pairs={{2,0},{4,2},{6,4},{8,6},{10,8},{12,10},{14,12},{16,14},{18,16},{20... | collective-permute-start | bytes 184328 | tf_op jit(solution)/shard_map/ppermute | solution.py:26
  51.4 4.5 %collective-permute-start.3 = (f32[15,1024]{1,0:T(8,128)S(1)}, f32[15,1024]{1,0:T(8,128)S(1)}, u32[]{:S(2)}, u32[]{:S(2)}) collective-permute-start(f32[15,1024]{1,0:T(8,128)S(1)} %get-tuple-element.51), channel_id=1, source_target_pairs={{0,2},{2,4},{4,6},{6,8},{8,10},{10,12},{12,14},{14,16},{16,18},{18... | collective-permute-start | bytes 184328 | tf_op jit(solution)/shard_map/ppermute | solution.py:23
  56.0 0.0 collective-permute-done.5
  56.0 1.6 %collective-permute-start.6 = (f32[33,1024]{1,0:T(8,128)S(1)}, f32[33,1024]{1,0:T(8,128)}, u32[]{:S(2)}, u32[]{:S(2)}) collective-permute-start(f32[33,1024]{1,0:T(8,128)S(1)} %add.291), channel_id=1, source_target_pairs={{0,8},{2,10},{4,12},{6,14},{8,0},{10,2},{12,4},{14,6},{16,24},{18,... | collective-permute-start | bytes 405512 | tf_op jit(solution)/shard_map/ppermute | solution.py:14
  57.6 0.0 collective-permute-done.2
  57.6 0.2 collective-permute-done.3
  57.8 0.0 copy-done.1
  57.8 6.6 %fusion.4 = (bf16[256,1024]{1,0:T(8,128)(2,1)}, f32[256,1024]{1,0:T(8,128)}) fusion(bf16[256,1024]{1,0:T(8,128)(2,1)S(1)} %copy-done.3, bf16[256,1024]{1,0:T(8,128)(2,1)S(1)} %copy-done.1, f32[256,1024]{1,0:T(8,128)S(1)} %get-tuple-element.46, f32[15,1024]{1,0:T(8,128)S(1)} %collective-permute-done.3, f32[1024]{0:T(1024)} %bitcast.127, f32[1024]{0:T(1024)} %bitcast.129, ...), kind=kLoop, calls=%fused_computation.35 | loop fusion | flops 26476544 | bytes 3919872 | tf_op jit(solution)/shard_map/convert_element_type | solution.py:97
  64.4 0.0 collective-permute-done.6
  64.4 0.9 %add.292 = f32[33,1024]{1,0:T(8,128)S(1)} add(f32[33,1024]{1,0:T(8,128)S(1)} %add.291, f32[33,1024]{1,0:T(8,128)} %collective-permute-done.6) | non-fusion elementwise | flops 33792 | bytes 405504 | tf_op jit(solution)/shard_map/add | solution.py:14
  65.4 5.9 %collective-permute-start.7 = (f32[33,1024]{1,0:T(8,128)S(1)}, f32[33,1024]{1,0:T(8,128)S(1)}, u32[]{:S(2)}, u32[]{:S(2)}) collective-permute-start(f32[33,1024]{1,0:T(8,128)S(1)} %add.292), channel_id=1, source_target_pairs={{0,16},{2,18},{4,20},{6,22},{8,24},{10,26},{12,28},{14,30},{16,0},... | collective-permute-start | bytes 405512 | tf_op jit(solution)/shard_map/ppermute | solution.py:14
  71.2 2.3 %multiply_convert_fusion = bf16[256,1024]{1,0:T(8,128)(2,1)} fusion(f32[256,1024]{1,0:T(8,128)} %get-tuple-element.48, bf16[256,1024]{1,0:T(8,128)(2,1)S(1)} %copy-done.1), kind=kLoop, calls=%fused_computation.182 | loop fusion | flops 1572864 | bytes 2097152 | tf_op jit(solution)/shard_map/convert_element_type | solution.py:96
  73.5 3.5 %collective-permute-done.7 = f32[33,1024]{1,0:T(8,128)S(1)} collective-permute-done((f32[33,1024]{1,0:T(8,128)S(1)}, f32[33,1024]{1,0:T(8,128)S(1)}, u32[]{:S(2)}, u32[]{:S(2)}) %collective-permute-start.7) | collective-permute-done | bytes 135200 | tf_op jit(solution)/shard_map/ppermute | solution.py:14
  77.0 0.6 fusion.97
  77.6 0.7 slice.579
  (12 shorter events, 0.2 us)
Async XLA Ops:
  0.6 20.8 %copy-start = (bf16[256,2048]{1,0:T(8,128)(2,1)S(1)}, bf16[256,2048]{1,0:T(8,128)(2,1)}, u32[]{:S(2)}) copy-start(bf16[256,2048]{1,0:T(8,128)(2,1)} %param.13) | copy-start | bytes 3145732
  0.6 7.8 %copy-start.4 = (f32[31,1024]{1,0:T(8,128)S(1)}, f32[31,1024]{1,0:T(8,128)}, u32[]{:S(2)}) copy-start(f32[31,1024]{1,0:T(8,128)} %param.9) | copy-start | bytes 380932
  2.3 6.5 %collective-permute-start = (bf16[15,1024]{1,0:T(8,128)(2,1)S(1)}, bf16[15,1024]{1,0:T(8,128)(2,1)S(1)}, u32[]{:S(2)}, u32[]{:S(2)}) collective-permute-start(bf16[15,1024]{1,0:T(8,128)(2,1)S(1)} %get-tuple-element.52), channel_id=1, source_target_pairs={{0,2},{2,4},{4,6},{6,8},{8,10},{10,12},{12,14},{14,16},{16,18},{18... | collective-permute-start | bytes 92168 | tf_op jit(solution)/shard_map/ppermute | solution.py:23
  7.2 5.8 %collective-permute-start.1 = (bf16[15,1024]{1,0:T(8,128)(2,1)S(1)}, bf16[15,1024]{1,0:T(8,128)(2,1)S(1)}, u32[]{:S(2)}, u32[]{:S(2)}) collective-permute-start(bf16[15,1024]{1,0:T(8,128)(2,1)S(1)} %get-tuple-element.53), channel_id=1, source_target_pairs={{2,0},{4,2},{6,4},{8,6},{10,8},{12,10},{14,12},{16,14},{18,16},{20... | collective-permute-start | bytes 92168 | tf_op jit(solution)/shard_map/ppermute | solution.py:26
  8.6 10.3 %copy-start.5 = (f32[1,1024]{1,0:T(1,128)}, f32[1,1024]{1,0:T(1,128)S(1)}, u32[]{:S(2)}) copy-start(f32[1,1024]{1,0:T(1,128)S(1)} %get-tuple-element.84) | copy-start | bytes 12292
  8.6 10.3 %copy-start.6 = (f32[1,1024]{1,0:T(1,128)}, f32[1,1024]{1,0:T(1,128)S(1)}, u32[]{:S(2)}) copy-start(f32[1,1024]{1,0:T(1,128)S(1)} %get-tuple-element.85) | copy-start | bytes 12292
  8.6 10.3 %copy-start.7 = (f32[1,1024]{1,0:T(1,128)}, f32[1,1024]{1,0:T(1,128)S(1)}, u32[]{:S(2)}) copy-start(f32[1,1024]{1,0:T(1,128)S(1)} %get-tuple-element.86) | copy-start | bytes 12292
  13.1 8.2 %copy-start.8 = (f32[1024]{0:T(1024)S(1)}, f32[1024]{0:T(1024)}, u32[]{:S(2)}) copy-start(f32[1024]{0:T(1024)} %param.10) | copy-start | bytes 12292
  13.2 8.2 %copy-start.9 = (f32[1024]{0:T(1024)S(1)}, f32[1024]{0:T(1024)}, u32[]{:S(2)}) copy-start(f32[1024]{0:T(1024)} %param.11) | copy-start | bytes 12292
  18.9 8.0 %copy-start.2 = (f32[256,1024]{1,0:T(8,128)}, f32[256,1024]{1,0:T(8,128)S(1)}, u32[]{:S(2)}) copy-start(f32[256,1024]{1,0:T(8,128)S(1)} %get-tuple-element.49) | copy-start | bytes 3145732
  36.6 21.2 %copy-start.1 = (bf16[256,1024]{1,0:T(8,128)(2,1)S(1)}, bf16[256,1024]{1,0:T(8,128)(2,1)}, u32[]{:S(2)}) copy-start(bf16[256,1024]{1,0:T(8,128)(2,1)} %param.8) | copy-start | bytes 1572868
  36.6 21.2 %copy-start.3 = (bf16[256,1024]{1,0:T(8,128)(2,1)S(1)}, bf16[256,1024]{1,0:T(8,128)(2,1)}, u32[]{:S(2)}) copy-start(bf16[256,1024]{1,0:T(8,128)(2,1)} %param.7) | copy-start | bytes 1572868
  40.6 7.0 %collective-permute-start.4 = (f32[33,1024]{1,0:T(8,128)S(1)}, f32[33,1024]{1,0:T(8,128)S(1)}, u32[]{:S(2)}, u32[]{:S(2)}) collective-permute-start(f32[33,1024]{1,0:T(8,128)S(1)} %broadcast_multiply_fusion), channel_id=1, source_target_pairs={{0,2},{2,0},{4,6},{6,4},{8,10},{10,8},{12,14},{14,12},{16,18},{18,... | collective-permute-start | bytes 405512 | tf_op jit(solution)/shard_map/ppermute | solution.py:14
  47.6 8.4 %collective-permute-start.5 = (f32[33,1024]{1,0:T(8,128)S(1)}, f32[33,1024]{1,0:T(8,128)S(1)}, u32[]{:S(2)}, u32[]{:S(2)}) collective-permute-start(f32[33,1024]{1,0:T(8,128)S(1)} %fusion.93), channel_id=1, source_target_pairs={{0,4},{2,6},{4,0},{6,2},{8,12},{10,14},{12,8},{14,10},{16,20},{18,... | collective-permute-start | bytes 405512 | tf_op jit(solution)/shard_map/ppermute | solution.py:14
  50.1 7.5 %collective-permute-start.2 = (f32[15,1024]{1,0:T(8,128)S(1)}, f32[15,1024]{1,0:T(8,128)S(1)}, u32[]{:S(2)}, u32[]{:S(2)}) collective-permute-start(f32[15,1024]{1,0:T(8,128)S(1)} %get-tuple-element.50), channel_id=1, source_target_pairs={{2,0},{4,2},{6,4},{8,6},{10,8},{12,10},{14,12},{16,14},{18,16},{20... | collective-permute-start | bytes 184328 | tf_op jit(solution)/shard_map/ppermute | solution.py:26
  51.4 6.4 %collective-permute-start.3 = (f32[15,1024]{1,0:T(8,128)S(1)}, f32[15,1024]{1,0:T(8,128)S(1)}, u32[]{:S(2)}, u32[]{:S(2)}) collective-permute-start(f32[15,1024]{1,0:T(8,128)S(1)} %get-tuple-element.51), channel_id=1, source_target_pairs={{0,2},{2,4},{4,6},{6,8},{8,10},{10,12},{12,14},{14,16},{16,18},{18... | collective-permute-start | bytes 184328 | tf_op jit(solution)/shard_map/ppermute | solution.py:23
  56.0 8.4 %collective-permute-start.6 = (f32[33,1024]{1,0:T(8,128)S(1)}, f32[33,1024]{1,0:T(8,128)}, u32[]{:S(2)}, u32[]{:S(2)}) collective-permute-start(f32[33,1024]{1,0:T(8,128)S(1)} %add.291), channel_id=1, source_target_pairs={{0,8},{2,10},{4,12},{6,14},{8,0},{10,2},{12,4},{14,6},{16,24},{18,... | collective-permute-start | bytes 405512 | tf_op jit(solution)/shard_map/ppermute | solution.py:14
  65.4 11.6 %collective-permute-start.7 = (f32[33,1024]{1,0:T(8,128)S(1)}, f32[33,1024]{1,0:T(8,128)S(1)}, u32[]{:S(2)}, u32[]{:S(2)}) collective-permute-start(f32[33,1024]{1,0:T(8,128)S(1)} %add.292), channel_id=1, source_target_pairs={{0,16},{2,18},{4,20},{6,22},{8,24},{10,26},{12,28},{14,30},{16,0},... | collective-permute-start | bytes 405512 | tf_op jit(solution)/shard_map/ppermute | solution.py:14
